TPU v7x, 32 devices: a whole 2x2x4 slice. The times are simulated.
32 devices in a mesh: fs: 8 (over z, core), tp: 4 (over y, x).
Axes of the slice: x: 2, y: 2, z: 4, core: 2. Of those that a mesh axis runs over, the one named last changes fastest.
Arguments:
- tokens: bfloat16 [4096, 4096], P('fs', 'tp'), may hold values from -16 to 16
- norm_gain: float32 [4096], P('fs'), may hold values from 0.1 to 1.9
- gate_train: float32 [4096, 12288], P('fs', 'tp'), may hold values from -6 to 6
- up_train: float32 [4096, 12288], P('fs', 'tp'), may hold values from -6 to 6
Outputs:
- gate_serve: bfloat16 [4096, 12288], P(None, 'tp')
- up_serve: bfloat16 [4096, 12288], P(None, 'tp')
- hidden: bfloat16 [4096, 12288], P('fs', 'tp')
All inputs are finite; a program needn't handle non-finite values.
Results may differ from a plain program's by a relative error of at most 0.0071.
Values may be sent and summed in bfloat16 or wider, within the bound.
A program may use at most 192 MiB of HBM per device.

v0:
```python
import jax
import jax.numpy as jnp
from jax import lax
from jax.sharding import PartitionSpec as P


def body(tokens, norm_gain, gate_train, up_train):
    gain = norm_gain[:, None]
    gate_local = (gate_train * gain).astype(jnp.bfloat16)
    up_local = (up_train * gain).astype(jnp.bfloat16)
    whole = lax.all_gather(tokens, "tp", axis=1, tiled=True)
    values = whole.astype(jnp.float32)
    normed = (values * lax.rsqrt(jnp.mean(values * values, axis=-1, keepdims=True) + 1e-06)).astype(
        jnp.bfloat16
    )
    width = normed.shape[1]
    scale = width ** (-0.5)
    gate_serve, up_serve = (
        lax.all_gather(gate_local, "fs", axis=0, tiled=True),
        lax.all_gather(up_local, "fs", axis=0, tiled=True),
    )
    gate_acc = jnp.dot(normed, gate_serve, preferred_element_type=jnp.float32)
    up_acc = jnp.dot(normed, up_serve, preferred_element_type=jnp.float32)
    gate = gate_acc * scale
    up = up_acc * scale
    hidden = (jax.nn.silu(gate) * up).astype(jnp.bfloat16)
    return (gate_serve, up_serve, hidden)


def solution(mesh):
    in_specs = (P("fs", "tp"), P("fs"), P("fs", "tp"), P("fs", "tp"))
    out_specs = (P(None, "tp"), P(None, "tp"), P("fs", "tp"))
    return jax.shard_map(body, mesh=mesh, in_specs=in_specs, out_specs=out_specs, check_vma=False)
```

profile of v0, /device:TPU:0, one launch (start us, length us, event | category | flops | bytes accessed | tf_op | source)
XLA Modules:
  0.0 569.7 jit_solution(12411793271498854987)
XLA Ops:
  7.2 0.0 all-gather.8.cloned.1.call-start
  7.2 0.7 all-gather.8.cloned.1.call-update
  7.9 0.0 all-gather.4.cloned.1.call-start
  7.9 9.3 %multiply_convert_fusion.1 = (bf16[512,3072]{1,0:T(8,128)(2,1)}, bf16[512,3072]{1,0:T(8,128)(2,1)}) fusion(f32[512,3072]{1,0:T(8,128)} %param.7, f32[512]{0:T(512)} %param.5, f32[512,3072]{1,0:T(8,128)} %param.6), kind=kLoop, calls=%fused_computation.5 | loop fusion | flops 6291456 | bytes 18876416 | tf_op jit(solution)/shard_map/convert_element_type | solution.py:10
  17.2 0.0 all-gather.4.cloned.1.call-update
  17.3 0.0 all-gather.6.cloned.1.call-start
  17.3 0.7 all-gather.6.cloned.1.call-update
  18.0 47.2 %all-gather.8.cloned.1.call-done = bf16[512,4096]{1,0:T(8,128)(2,1)} async-done(((bf16[512,1024]{1,0:T(8,128)(2,1)}), bf16[512,4096]{1,0:T(8,128)(2,1)}) %all-gather.8.cloned.1.call-update) | async-done | bytes 4194320 | tf_op jit(solution)/shard_map/all_gather | solution.py:11
  65.1 3.1 fusion
  68.2 219.0 %all-gather.4.cloned.1.call-done = bf16[4096,3072]{1,0:T(8,128)(2,1)} async-done(((bf16[512,3072]{1,0:T(8,128)(2,1)}), bf16[4096,3072]{1,0:T(8,128)(2,1)}) %all-gather.4.cloned.1.call-update) | async-done | bytes 25165840 | tf_op jit(solution)/shard_map/all_gather | solution.py:19
  287.2 20.6 %fusion.3 = f32[512,3072]{1,0:T(8,128)} fusion(bf16[4096,3072]{1,0:T(8,128)(2,1)} %all-gather.4.cloned.1.call-done, bf16[512,4096]{1,0:T(8,128)(2,1)} %all-gather.8.cloned.1.call-done, f32[512]{0:T(512)S(1)} %add_rsqrt_fusion), kind=kOutput, calls=%fused_computation.7 | convolution fusion | flops 12891193344 | bytes 35653632 | tf_op jit(solution)/shard_map/dot_general | solution.py:22
  307.8 199.7 %all-gather.6.cloned.1.call-done = bf16[4096,3072]{1,0:T(8,128)(2,1)} async-done(((bf16[512,3072]{1,0:T(8,128)(2,1)}), bf16[4096,3072]{1,0:T(8,128)(2,1)}) %all-gather.6.cloned.1.call-update) | async-done | bytes 25165840 | tf_op jit(solution)/shard_map/all_gather | solution.py:20
  507.5 21.8 %multiply_convert_fusion = bf16[512,3072]{1,0:T(8,128)(2,1)} fusion(f32[512,3072]{1,0:T(8,128)} %fusion.3, bf16[4096,3072]{1,0:T(8,128)(2,1)} %all-gather.6.cloned.1.call-done, bf16[512,4096]{1,0:T(8,128)(2,1)} %all-gather.8.cloned.1.call-done, f32[512]{0:T(512)S(1)} %add_rsqrt_fusion), kind=kOutput, calls=%fused_computation.4 | convolution fusion | flops 12903776256 | bytes 38799360 | tf_op jit(solution)/shard_map/dot_general | solution.py:23
  529.4 0.0 copy-start
  529.4 22.0 %copy.9 = bf16[4096,3072]{1,0:T(8,128)(2,1)} copy(bf16[4096,3072]{1,0:T(8,128)(2,1)} %all-gather.4.cloned.1.call-done) | data formatting | bytes 50331648
  551.3 2.9 copy-done
  554.3 8.9 %copy.10 = bf16[4096,3072]{1,0:T(8,128)(2,1)} copy(bf16[4096,3072]{1,0:T(8,128)(2,1)S(1)} %copy-done) | data formatting | bytes 50331648
  (1 shorter events, 0.0 us)
Async XLA Ops:
  7.2 58.0 %all-gather.8.cloned.1.call-start = ((), (), s32[]{:S(2)}) async-start(), calls=%async_computation.2 | async-start | bytes 5242880 | tf_op jit(solution)/shard_map/all_gather | solution.py:11
  7.9 279.3 %all-gather.4.cloned.1.call-start = ((), (), s32[]{:S(2)}) async-start(), calls=%async_computation | async-start | bytes 28311552 | tf_op jit(solution)/shard_map/all_gather | solution.py:19
  17.3 490.3 %all-gather.6.cloned.1.call-start = ((), (), s32[]{:S(2)}) async-start(), calls=%async_computation.1 | async-start | bytes 28311552 | tf_op jit(solution)/shard_map/all_gather | solution.py:20
  529.4 24.9 %copy-start = (bf16[4096,3072]{1,0:T(8,128)(2,1)S(1)}, bf16[4096,3072]{1,0:T(8,128)(2,1)}, u32[]{:S(2)}) copy-start(bf16[4096,3072]{1,0:T(8,128)(2,1)} %all-gather.6.cloned.1.call-done) | copy-start | bytes 75497472
Sparse Core Ops, SparseCore 0:
  9.8 55.2 all-gather.7
  67.4 219.8 all-gather.3
  289.5 218.0 all-gather.5
where the time goes:
time: 570 us
  waiting for transfers between devices  467 us (82%)
  matrix products  42.4 us (7%)
  local copies, waits for them, and re-layouts  33.8 us (6%)
  between operations  13.7 us (2%)
  other arithmetic  12.4 us (2%)
    all_gather x1, waiting for transfers between devices, body(): lax.all_gather(gate_local, 'fs', axis=0, tiled=True)  219 us
    all_gather x1, waiting for transfers between devices, body(): lax.all_gather(up_local, 'fs', axis=0, tiled=True)  200 us
    all_gather x1, waiting for transfers between devices, body(): whole = lax.all_gather(tokens, 'tp', axis=1, tiled=True)  47.2 us
    unnamed x4, local copies, waits for them, and re-layouts  33.8 us
    dot_general x1, matrix products, body(): up_acc = jnp.dot(normed, up_serve, preferred_element_type=jnp.float32)  21.8 us
    dot_general x1, matrix products, body(): gate_acc = jnp.dot(normed, gate_serve, preferred_element_type=jnp.float32)  20.6 us
  transfers between devices with their start and end apart: 3, of which 3 were waited for; matrix products, arithmetic and copies ran while one was open for 6% of the time, Pallas kernels for 0%

commit v1 on v0

--- a/solution.py
+++ b/solution.py
@@ -1,7 +1,20 @@
+import functools
 import jax
 import jax.numpy as jnp
 from jax import lax
 from jax.sharding import PartitionSpec as P
+
+
+def see_desk(x_local, axis_tag):
+    return jnp.concatenate(
+        jax.lax.all_to_all(
+            jnp.stack(jax.lax.axis_size(axis_tag) * [x_local], axis=0), axis_tag, 0, 0
+        ),
+        axis=0,
+    )
+
+
+wait_streams_for = functools.partial(see_desk, axis_tag="fs")
 
 
 def body(tokens, norm_gain, gate_train, up_train):
@@ -16,7 +29,7 @@
     width = normed.shape[1]
     scale = width ** (-0.5)
     gate_serve, up_serve = (
-        lax.all_gather(gate_local, "fs", axis=0, tiled=True),
+        wait_streams_for(gate_local),
         lax.all_gather(up_local, "fs", axis=0, tiled=True),
     )
     gate_acc = jnp.dot(normed, gate_serve, preferred_element_type=jnp.float32)

time: 570 us -> 861 us (1.51)
  waiting for transfers between devices: 467 us -> 744 us
  local copies, waits for them, and re-layouts: 33.8 us -> 42.9 us
    all_to_all x0 -> x1, waiting for transfers between devices: none -> 710 us  [see_desk(): jax.lax.all_to_all(jnp.stack(jax.lax.axis_size(axis_tag) * [x_local], axi...]
    all_gather x1 -> x0, waiting for transfers between devices: 219 us -> none  [body(): lax.all_gather(gate_local, 'fs', axis=0, tiled=True)]
    all_gather x1, waiting for transfers between devices: 200 us -> 0.01 us  [body(): lax.all_gather(up_local, 'fs', axis=0, tiled=True)]
    all_gather x1, waiting for transfers between devices: 47.2 us -> 32.8 us  [body(): whole = lax.all_gather(tokens, 'tp', axis=1, tiled=True)]
    another operation x0 -> x1, local copies, waits for them, and re-layouts: none -> 9.05 us  [see_desk(): jnp.stack(jax.lax.axis_size(axis_tag) * [x_local], axis=0)]
  transfers between devices with their start and end apart: 3 -> 3, of which waited for: 3 -> 2; matrix products, arithmetic and copies ran while one was open for 6% -> 5% of each run, Pallas kernels for 0% -> 0%
where the time goes in v1:
time: 861 us; the launch traced here: 860 us
  waiting for transfers between devices  744 us (86%)
  local copies, waits for them, and re-layouts  42.9 us (5%)
  matrix products  41.5 us (5%)
  between operations  14.1 us (2%)
  other arithmetic  11.3 us (1%)
    all_to_all x1, waiting for transfers between devices, see_desk(): jax.lax.all_to_all(jnp.stack(jax.lax.axis_size(axis_tag) * [x_local], axi...  710 us
    unnamed x4, local copies, waits for them, and re-layouts  33.8 us
    all_gather x1, waiting for transfers between devices, body(): whole = lax.all_gather(tokens, 'tp', axis=1, tiled=True)  32.8 us
    dot_general x1, matrix products, body(): up_acc = jnp.dot(normed, up_serve, preferred_element_type=jnp.float32)  22 us
    dot_general x1, matrix products, body(): gate_acc = jnp.dot(normed, gate_serve, preferred_element_type=jnp.float32)  19.5 us
  transfers between devices with their start and end apart: 3, of which 2 were waited for; matrix products, arithmetic and copies ran while one was open for 5% of the time, Pallas kernels for 0%

profile of v1, /device:TPU:0, one launch (start us, length us, event | category | flops | bytes accessed | tf_op | source)
XLA Modules:
  0.0 860.3 jit_solution(1921243299904565065)
XLA Ops:
  7.2 0.0 all-gather.5.cloned.1.call-start
  7.2 0.7 all-gather.5.cloned.1.call-update
  7.9 8.2 multiply_convert_fusion.1
  16.1 9.1 %stack.2 = bf16[8,512,3072]{2,1,0:T(8,128)(2,1)} broadcast(bf16[512,3072]{1,0:T(8,128)(2,1)S(1)} %get-tuple-element.4), dimensions={1,2} | broadcast | bytes 28311552 | tf_op jit(solution)/shard_map/stack | solution.py:11
  25.2 6.4 all-to-all-start
  31.6 0.0 all-gather.3.cloned.1.call-start
  31.7 0.7 all-gather.3.cloned.1.call-update
  32.4 32.8 %all-gather.5.cloned.1.call-done = bf16[512,4096]{1,0:T(8,128)(2,1)} async-done(((bf16[512,1024]{1,0:T(8,128)(2,1)}), bf16[512,4096]{1,0:T(8,128)(2,1)}) %all-gather.5.cloned.1.call-update) | async-done | bytes 4194320 | tf_op jit(solution)/shard_map/all_gather | solution.py:24
  65.1 3.1 fusion
  68.2 709.9 %all-to-all-done = bf16[8,512,3072]{2,1,0:T(8,128)(2,1)} async-done(((bf16[8,512,3072]{2,1,0:T(8,128)(2,1)}), bf16[8,512,3072]{2,1,0:T(8,128)(2,1)}, u32[]{:S(2)}, u32[]{:S(2)}) %all-to-all-start) | async-done | bytes 25165856 | tf_op jit(solution)/shard_map/all_to_all | solution.py:10
  778.1 19.5 %fusion.3 = f32[512,3072]{1,0:T(8,128)} fusion(bf16[4096,3072]{1,0:T(8,128)(2,1)} %bitcast, bf16[512,4096]{1,0:T(8,128)(2,1)} %all-gather.5.cloned.1.call-done, f32[512]{0:T(512)S(1)} %add_rsqrt_fusion), kind=kOutput, calls=%fused_computation.7 | convolution fusion | flops 12891193344 | bytes 35653632 | tf_op jit(solution)/shard_map/dot_general | solution.py:35
  797.6 0.0 all-gather.3.cloned.1.call-done
  797.6 22.0 %multiply_convert_fusion = bf16[512,3072]{1,0:T(8,128)(2,1)} fusion(f32[512,3072]{1,0:T(8,128)} %fusion.3, bf16[4096,3072]{1,0:T(8,128)(2,1)} %all-gather.3.cloned.1.call-done, bf16[512,4096]{1,0:T(8,128)(2,1)} %all-gather.5.cloned.1.call-done, f32[512]{0:T(512)S(1)} %add_rsqrt_fusion), kind=kOutput, calls=%fused_computation.4 | convolution fusion | flops 12903776256 | bytes 38799360 | tf_op jit(solution)/shard_map/dot_general | solution.py:36
  819.6 0.0 copy-start
  819.6 22.0 %copy.9 = bf16[4096,3072]{1,0:T(8,128)(2,1)} copy(bf16[4096,3072]{1,0:T(8,128)(2,1)} %bitcast) | data formatting | bytes 50331648
  841.6 2.9 copy-done
  844.5 8.9 %copy.10 = bf16[4096,3072]{1,0:T(8,128)(2,1)} copy(bf16[4096,3072]{1,0:T(8,128)(2,1)S(1)} %copy-done) | data formatting | bytes 50331648
  (1 shorter events, 0.0 us)
Async XLA Ops:
  7.2 58.0 %all-gather.5.cloned.1.call-start = ((), (), s32[]{:S(2)}) async-start(), calls=%async_computation.2 | async-start | bytes 5242880 | tf_op jit(solution)/shard_map/all_gather | solution.py:24
  25.2 752.9 %all-to-all-start = ((bf16[8,512,3072]{2,1,0:T(8,128)(2,1)}), bf16[8,512,3072]{2,1,0:T(8,128)(2,1)}, u32[]{:S(2)}, u32[]{:S(2)}) async-start(bf16[8,512,3072]{2,1,0:T(8,128)(2,1)} %stack.2), calls=%async_computation | async-start | bytes 50331648 | tf_op jit(solution)/shard_map/all_to_all | solution.py:10
  31.6 766.0 %all-gather.3.cloned.1.call-start = ((), (), s32[]{:S(2)}) async-start(), calls=%async_computation.1 | async-start | bytes 28311552 | tf_op jit(solution)/shard_map/all_gather | solution.py:33
  819.6 24.9 %copy-start = (bf16[4096,3072]{1,0:T(8,128)(2,1)S(1)}, bf16[4096,3072]{1,0:T(8,128)(2,1)}, u32[]{:S(2)}) copy-start(bf16[4096,3072]{1,0:T(8,128)(2,1)} %all-gather.3.cloned.1.call-done) | copy-start | bytes 75497472
Sparse Core Ops, SparseCore 0:
  9.8 55.2 all-gather.4
  67.4 438.7 all-gather.2
